TPU v7x, 32 devices: a whole 2x2x4 slice. The times are simulated.
32 devices in a mesh: sp: 8 (over z, y), tp: 4 (over x, core).
Axes of the slice: x: 2, y: 2, z: 4, core: 2. Of those that a mesh axis runs over, the one named last changes fastest.
Arguments:
- latent: bfloat16 [4096, 2048], P(('sp', 'tp')), may hold values from -6 to 6
- context: bfloat16 [512, 2048], P('sp'), may hold values from -6 to 6
- condition: float32 [2048], replicated, may hold values from -6 to 6
- context_condition: float32 [2048], replicated, may hold values from -6 to 6
- norm_gain: float32 [2048], replicated, may hold values from 0.1 to 1.9
- shift_weight: bfloat16 [2048, 2048], P('sp', 'tp'), may hold values from -0.21875 to 0.21875
- scale_weight: bfloat16 [2048, 2048], P('sp', 'tp'), may hold values from -0.21875 to 0.21875
- gate_weight: bfloat16 [2048, 2048], P('sp', 'tp'), may hold values from -0.21875 to 0.21875
- query_weight: bfloat16 [2048, 1024], P(None, 'tp'), may hold values from -1 to 1
- key_weight: bfloat16 [2048, 512], P(None, 'tp'), may hold values from -1 to 1
- value_weight: bfloat16 [2048, 512], P(None, 'tp'), may hold values from -0.125 to 0.125
- query_gain: float32 [64], replicated, may hold values from 0.1 to 7.8
- key_gain: float32 [64], replicated, may hold values from 0.1 to 7.8
- output_weight: bfloat16 [1024, 2048], replicated, may hold values from -1 to 1
Outputs:
- updated: bfloat16 [4096, 2048], P(('sp', 'tp'))
All inputs are finite; a program needn't handle non-finite values.
Results may differ from a plain program's by a relative error of at most 0.012.
The roundings to bfloat16 on the way count: a program that leaves them out, or rounds other values in their place, can miss the bound.
Values may be sent and summed in bfloat16 or wider, within the bound.
A program may use at most 64 MiB of HBM per device.

v0:
```python
import math
import jax
import jax.numpy as jnp
from jax import lax
from jax.sharding import PartitionSpec as P

CHANNEL_SPAN = 64
GRID_W = 64
epsilon = 1e-06
rope_base = 10000.0


def modulate(tok_rows, norm_gain, shift_row, scale_row):
    wide = tok_rows.astype(jnp.float32)
    normed = wide * lax.rsqrt(jnp.mean(wide * wide, axis=-1, keepdims=True) + epsilon)
    return (normed * norm_gain * (1.0 + scale_row) + shift_row).astype(jnp.bfloat16)


def headnorm(raw, gain, heads):
    field = raw.reshape(raw.shape[0], heads, -1)
    return field * lax.rsqrt(jnp.mean(field * field, axis=-1, keepdims=True) + epsilon) * gain


def rotate(field, places):
    count = field.shape[0]
    heads = field.shape[1]
    quarter = field.shape[2] // 4
    grid_row = (places // GRID_W).astype(jnp.float32)
    grid_col = (places % GRID_W).astype(jnp.float32)
    inverse = rope_base ** (-jnp.arange(quarter, dtype=jnp.float32) / quarter)
    angles = jnp.stack([grid_row[:, None] * inverse, grid_col[:, None] * inverse], axis=1)[:, None]
    cosine = jnp.cos(angles)
    sine = jnp.sin(angles)
    matcher_content_couples = field.reshape(count, heads, 2, 2, quarter)
    first = matcher_content_couples[:, :, :, 0]
    second = matcher_content_couples[:, :, :, 1]
    turned = jnp.stack([first * cosine - second * sine, second * cosine + first * sine], axis=3)
    return turned.reshape(count, heads, 4 * quarter)


def process_probe_group(
    accumulator_carry, probe_entries, matcher_content_couples, similarity_offset
):
    row_peak, row_total, weighted = accumulator_carry
    kv_heads = probe_entries.shape[1]
    head_size = probe_entries.shape[3]
    pair_width = kv_heads * head_size
    matcher_pieces = matcher_content_couples[:, :pair_width].reshape(
        matcher_content_couples.shape[0], kv_heads, head_size
    )
    value_rows = matcher_content_couples[:, pair_width:].reshape(
        matcher_content_couples.shape[0], kv_heads, head_size
    )
    similarity_matrix = (
        jnp.einsum(
            "dmvk,hmk->dmvh", probe_entries, matcher_pieces, preferred_element_type=jnp.float32
        )
        * head_size ** (-0.5)
        + similarity_offset
    )
    new_peak = jnp.maximum(row_peak, jnp.max(similarity_matrix, axis=-1))
    shares = jnp.exp(similarity_matrix - new_peak[..., None])
    shrink = jnp.exp(row_peak - new_peak)
    row_total = row_total * shrink + jnp.sum(shares, axis=-1)
    weighted = weighted * shrink[..., None] + jnp.einsum(
        "qkgn,nkd->qkgd",
        shares.astype(jnp.bfloat16),
        value_rows,
        preferred_element_type=jnp.float32,
    )
    return (new_peak, row_total, weighted)


def group_walker(accumulator_carry, probe_entries, matcher_content_couples, similarity_offset):
    pair_count = matcher_content_couples.shape[0]
    probe_group_total = -(-pair_count // 2048)
    while pair_count % probe_group_total:
        probe_group_total += 1
    if probe_group_total == 1:
        return process_probe_group(
            accumulator_carry, probe_entries, matcher_content_couples, similarity_offset
        )
    group_extent = pair_count // probe_group_total

    def scan_step(inner, slices):
        return (process_probe_group(inner, probe_entries, slices[0], slices[1]), None)

    result, unused = lax.scan(
        scan_step,
        accumulator_carry,
        (
            matcher_content_couples.reshape(
                probe_group_total, group_extent, matcher_content_couples.shape[1]
            ),
            similarity_offset.reshape(probe_group_total, group_extent),
        ),
    )
    return result


def on_device(
    latent,
    context,
    condition,
    context_condition,
    norm_gain,
    shift_weight,
    scale_weight,
    gate_weight,
    query_weight,
    key_weight,
    value_weight,
    query_gain,
    key_gain,
    output_weight,
):
    head_split = lax.axis_size("tp")
    seq_index = lax.axis_index("sp")
    head_index = lax.axis_index("tp")
    row_slab = shift_weight.shape[0]
    columns = shift_weight.shape[1]
    conditions = jnp.stack([condition, context_condition])
    activated = jax.nn.silu(
        lax.dynamic_slice_in_dim(conditions, seq_index * row_slab, row_slab, 1)
    ).astype(jnp.bfloat16)
    part_shift = jnp.dot(activated, shift_weight, preferred_element_type=jnp.float32)
    part_scale = jnp.dot(activated, scale_weight, preferred_element_type=jnp.float32)
    part_gate = jnp.dot(activated, gate_weight, preferred_element_type=jnp.float32)

    def widen(member):
        blank = jnp.zeros((2, columns * head_split), jnp.float32)
        return lax.dynamic_update_slice_in_dim(blank, member, head_index * columns, 1)

    shifts, scales, gates = lax.psum(
        (widen(part_shift), widen(part_scale), widen(part_gate)), ("sp", "tp")
    )
    own_rows = latent.shape[0]
    tok_count = own_rows * head_split
    ctx_rows = context.shape[0]
    hidden = modulate(latent, norm_gain, shifts[0], scales[0])
    context_hidden = modulate(context, norm_gain, shifts[1], scales[1])
    q_heads = query_weight.shape[1] // CHANNEL_SPAN
    kv_heads = key_weight.shape[1] // CHANNEL_SPAN
    group_size = q_heads // kv_heads
    q_width = q_heads * CHANNEL_SPAN
    kv_width = kv_heads * CHANNEL_SPAN
    joined_weight = jnp.concatenate([query_weight, key_weight, value_weight], axis=1)
    projected = jnp.dot(
        lax.all_gather(hidden, "tp", axis=0, tiled=True),
        joined_weight,
        preferred_element_type=jnp.float32,
    )
    places = seq_index * tok_count + jnp.arange(tok_count, dtype=jnp.int32)
    probe_entries = rotate(headnorm(projected[:, :q_width], query_gain, q_heads), places).astype(
        jnp.bfloat16
    )
    probe_entries = probe_entries.reshape(tok_count, kv_heads, group_size, CHANNEL_SPAN)
    latent_keys = rotate(
        headnorm(projected[:, q_width : q_width + kv_width], key_gain, kv_heads), places
    ).astype(jnp.bfloat16)
    latent_values = projected[:, q_width + kv_width :].astype(jnp.bfloat16)
    own_pairs = jnp.concatenate([latent_keys.reshape(tok_count, kv_width), latent_values], axis=1)
    ctx_projected = jnp.dot(
        context_hidden, joined_weight[:, q_width:], preferred_element_type=jnp.float32
    )
    ctx_keys = (
        headnorm(ctx_projected[:, :kv_width], key_gain, kv_heads)
        .astype(jnp.bfloat16)
        .reshape(ctx_rows, kv_width)
    )
    ctx_pairs = jnp.concatenate(
        [ctx_keys, ctx_projected[:, kv_width:].astype(jnp.bfloat16)], axis=1
    )
    prefix_mapped = math.log(tok_count / (2.0 * ctx_rows))
    stat_shape = (tok_count, kv_heads, group_size)
    start_state = (
        jnp.full(stat_shape, -jnp.inf, jnp.float32),
        jnp.zeros(stat_shape, jnp.float32),
        jnp.zeros(stat_shape + (CHANNEL_SPAN,), jnp.float32),
    )
    ctx_whole = lax.all_gather(ctx_pairs, "sp", axis=0, tiled=True)
    ctx_state = group_walker(
        start_state,
        probe_entries,
        ctx_whole,
        jnp.full((ctx_whole.shape[0],), prefix_mapped, jnp.float32),
    )
    key_piece = lax.all_gather(own_pairs, "sp", axis=0, tiled=True)
    final_state = group_walker(
        ctx_state, probe_entries, key_piece, jnp.zeros((key_piece.shape[0],), jnp.float32)
    )
    row_peak, row_total, weighted = final_state
    attended = (weighted / row_total[..., None]).astype(jnp.bfloat16).reshape(tok_count, q_width)
    branch = jnp.dot(
        lax.all_to_all(attended, "tp", split_axis=0, concat_axis=1, tiled=True),
        output_weight,
        preferred_element_type=jnp.float32,
    )
    return (latent.astype(jnp.float32) + gates[0] * branch).astype(jnp.bfloat16)


def solution(mesh):
    in_specs = (
        P(("sp", "tp"), None),
        P("sp", None),
        P(),
        P(),
        P(),
        P("sp", "tp"),
        P("sp", "tp"),
        P("sp", "tp"),
        P(None, "tp"),
        P(None, "tp"),
        P(None, "tp"),
        P(),
        P(),
        P(),
    )
    out_specs = P(("sp", "tp"), None)
    return jax.shard_map(
        on_device, mesh=mesh, in_specs=in_specs, out_specs=out_specs, check_vma=False
    )
```

profile of v0, /device:TPU:0, one launch (start us, length us, event | category | flops | bytes accessed | tf_op | source)
XLA Modules:
  0.0 205.1 jit_solution(11449940155735415239)
XLA Ops:
  6.5 1.3 fusion.31
  7.8 0.9 convolution_dynamic-update-slice_fusion.1
  8.8 1.2 convolution_dynamic-update-slice_fusion
  10.0 1.2 convolution_dynamic-update-slice_fusion.2
  11.2 42.4 %all-reduce = (f32[2,2048]{1,0:T(2,128)S(1)}, f32[2,2048]{1,0:T(2,128)S(1)}, f32[2,2048]{1,0:T(2,128)S(1)}) all-reduce(f32[2,2048]{1,0:T(2,128)S(1)} %convolution_dynamic-update-slice_fusion, f32[2,2048]{1,0:T(2,128)S(1)} %convolution_dynamic-update-slice_fusion.1, ...), channel_id=1, replica_groups=mesh['sp'=8,'tp'=4] {'sp','tp'}, use_global_device_ids=true, to_apply=%region_3.4 | all-reduce | flops 12288 | bytes 98304 | tf_op jit(solution)/shard_map/psum | solution.py:134
  53.6 2.1 %fusion.35 = bf16[128,2048]{1,0:T(8,128)(2,1)} fusion(bf16[128,2048]{1,0:T(8,128)(2,1)} %param.16, f32[2048]{0:T(1024)S(1)} %bitcast.136, f32[2048]{0:T(1024)S(1)} %bitcast.135, f32[2048]{0:T(1024)} %param.20, f32[128]{0:T(128)S(1)} %add_rsqrt_fusion.3), kind=kLoop, calls=%fused_computation.40 | loop fusion | flops 1572864 | bytes 1073664 | tf_op jit(solution)/shard_map/convert_element_type | solution.py:16
  55.8 0.7 mul.374
  56.7 0.2 fusion.51
  56.9 1.1 fusion.40
  58.1 20.3 %all-gather.3.cloned.1.call-done = bf16[512,2048]{1,0:T(8,128)(2,1)} async-done(((bf16[128,2048]{1,0:T(8,128)(2,1)}), bf16[512,2048]{1,0:T(8,128)(2,1)}) %all-gather.3.cloned.1.call-update) | async-done | bytes 2097168 | tf_op jit(solution)/shard_map/all_gather | solution.py:149
  78.3 3.5 %fusion.17 = f32[512,512]{0,1:T(8,128)S(1)} fusion(bf16[512,2048]{1,0:T(8,128)(2,1)} %all-gather.3.cloned.1.call-done, bf16[2048,128]{1,0:T(8,128)(2,1)} %param.26, bf16[2048,128]{1,0:T(8,128)(2,1)} %param.25, bf16[2048,256]{1,0:T(8,128)(2,1)} %param.24), kind=kOutput, calls=%fused_computation.22 | convolution fusion | flops 1080033280 | bytes 5242880 | tf_op jit(solution)/shard_map/dot_general | solution.py:148
  82.1 0.7 pad_maximum_fusion.1
  83.1 0.3 fusion.36
  83.5 0.1 reduce_sum.64
  83.7 0.1 mul.333
  84.0 31.9 %all_gather.9 = bf16[512,256]{1,0:T(8,128)(2,1)S(1)} all-gather(bf16[64,256]{1,0:T(8,128)(2,1)S(1)} %pad_maximum_fusion.4), channel_id=1, replica_groups=mesh['sp'=8,'tp'=4] {'sp'}, dimensions={0}, use_global_device_ids=true | all-gather | bytes 294912 | tf_op jit(solution)/shard_map/all_gather | solution.py:181
  116.5 0.8 bitcast_reduce_fusion.1
  117.2 0.8 fusion.14
  118.1 1.0 fusion.28
  119.1 15.0 %all-gather.5.cloned.1.call-done = bf16[4096,256]{0,1:T(8,128)(2,1)} async-done(((bf16[512,256]{0,1:T(8,128)(2,1)}), bf16[4096,256]{0,1:T(8,128)(2,1)}) %all-gather.5.cloned.1.call-update) | async-done | bytes 2097168 | tf_op jit(solution)/shard_map/all_gather | solution.py:188
  134.1 1.7 copy.61
  135.8 48.4 %while.14 = (s32[]{:T(128)}, f32[512,2,2]{0,2,1:T(2,128)S(1)}, f32[512,2,2]{0,2,1:T(2,128)S(1)}, f32[512,2,2,64]{0,3,2,1:T(8,128)S(1)}, bf16[2,2048,256]{1,2,0:T...) while((s32[]{:T(128)}, f32[512,2,2]{0,2,1:T(2,128)S(1)}, f32[512,2,2]{0,2,1:T(2,128)S(1)}, ...), condition=%wide.region_13.14_spmd, body=%wide.region_10.13_spmd.sunk | while | flops 1107562496 | bytes 57016408 | solution.py:88
  136.0 8.1 %bitcast_reduce_fusion.5 = (f32[512,2,2]{0,2,1:T(2,128)S(1)}, f32[2,2048,512,2]{2,1,3,0:T(8,128)}) fusion(bf16[2048,2,64,1]{0,2,3,1:T(8,128)(2,1)S(1)} %bitcast.116, bf16[512,2,2,64]{0,3,2,1:T(8,128)(2,1)S(1)} %get-tuple-element.187), kind=kOutput, calls=%fused_computation.1.clone.1 | convolution fusion | flops 545257472 | bytes 17571840 | tf_op jit(solution)/shard_map/while/body/eval_jaxpr/dmvk,hmk->dmvh/dot_general | solution.py:55
  144.1 8.5 %fusion.94 = f32[512,2,2]{0,2,1:T(2,128)S(1)} fusion(f32[2,2048,512,2]{2,1,3,0:T(8,128)} %get-tuple-element.164, f32[512,2,2]{0,2,1:T(2,128)S(1)} %max.4), kind=kLoop, calls=%fused_computation.4.clone.1 | loop fusion | flops 12580864 | bytes 16793600 | tf_op jit(solution)/shard_map/while/body/eval_jaxpr/reduce_sum | solution.py:64
  152.6 7.3 %fusion.95 = f32[512,2,2,64]{0,3,2,1:T(8,128)S(1)} fusion(bf16[2048,2,64,1]{0,2,3,1:T(8,128)(2,1)S(1)} %bitcast.117, f32[2,2048,512,2]{2,1,3,0:T(8,128)} %get-tuple-element.164, f32[512,2,2]{0,2,1:T(2,128)S(1)} %max.4, f32[512,2,2,64]{0,3,2,1:T(8,128)S(1)} %get-tuple-element.178, f32[512,2,2]{0,2,1:T(2,128)S(1)} %get-tuple-element.167), kind=kOutput, calls=%fused_computation.7.clone.1 | convolution fusion | flops 549715968 | bytes 18366464 | tf_op jit(solution)/shard_map/while/body/eval_jaxpr/qkgn,nkd->qkgd/dot_general | solution.py:65
  160.2 8.1 %bitcast_reduce_fusion.5 = (f32[512,2,2]{0,2,1:T(2,128)S(1)}, f32[2,2048,512,2]{2,1,3,0:T(8,128)}) fusion(bf16[2048,2,64,1]{0,2,3,1:T(8,128)(2,1)S(1)} %bitcast.116, bf16[512,2,2,64]{0,3,2,1:T(8,128)(2,1)S(1)} %get-tuple-element.187), kind=kOutput, calls=%fused_computation.1.clone.1 | convolution fusion | flops 545257472 | bytes 17571840 | tf_op jit(solution)/shard_map/while/body/eval_jaxpr/dmvk,hmk->dmvh/dot_general | solution.py:55
  168.3 8.5 %fusion.94 = f32[512,2,2]{0,2,1:T(2,128)S(1)} fusion(f32[2,2048,512,2]{2,1,3,0:T(8,128)} %get-tuple-element.164, f32[512,2,2]{0,2,1:T(2,128)S(1)} %max.4), kind=kLoop, calls=%fused_computation.4.clone.1 | loop fusion | flops 12580864 | bytes 16793600 | tf_op jit(solution)/shard_map/while/body/eval_jaxpr/reduce_sum | solution.py:64
  176.9 7.3 %fusion.95 = f32[512,2,2,64]{0,3,2,1:T(8,128)S(1)} fusion(bf16[2048,2,64,1]{0,2,3,1:T(8,128)(2,1)S(1)} %bitcast.117, f32[2,2048,512,2]{2,1,3,0:T(8,128)} %get-tuple-element.164, f32[512,2,2]{0,2,1:T(2,128)S(1)} %max.4, f32[512,2,2,64]{0,3,2,1:T(8,128)S(1)} %get-tuple-element.178, f32[512,2,2]{0,2,1:T(2,128)S(1)} %get-tuple-element.167), kind=kOutput, calls=%fused_computation.7.clone.1 | convolution fusion | flops 549715968 | bytes 18366464 | tf_op jit(solution)/shard_map/while/body/eval_jaxpr/qkgn,nkd->qkgd/dot_general | solution.py:65
  184.3 0.7 copy.51
  185.1 3.4 %all-to-all-start = ((bf16[4,128,256]{1,2,0:T(8,128)(2,1)}), bf16[4,128,256]{1,2,0:T(8,128)(2,1)S(1)}, u32[]{:S(2)}, u32[]{:S(2)}) async-start(bf16[4,128,256]{1,2,0:T(8,128)(2,1)} %copy.51), calls=%async_computation | async-start | bytes 524288 | tf_op jit(solution)/shard_map/all_to_all | solution.py:195
  188.5 6.0 %all-to-all-done = bf16[4,128,256]{1,2,0:T(8,128)(2,1)S(1)} async-done(((bf16[4,128,256]{1,2,0:T(8,128)(2,1)}), bf16[4,128,256]{1,2,0:T(8,128)(2,1)S(1)}, u32[]{:S(2)}, u32[]{:S(2)}) %all-to-all-start) | async-done | bytes 262176 | tf_op jit(solution)/shard_map/all_to_all | solution.py:195
  194.5 3.8 %fusion.16 = bf16[128,2048]{1,0:T(8,128)(2,1)} fusion(bf16[128,1024]{0,1:T(8,128)(2,1)S(1)} %bitcast.124, bf16[1024,2048]{1,0:T(8,128)(2,1)} %param.29, bf16[128,2048]{1,0:T(8,128)(2,1)} %param.16, f32[2048]{0:T(1024)S(1)} %bitcast.134), kind=kOutput, calls=%fused_computation.20 | convolution fusion | flops 537919488 | bytes 5513216 | tf_op jit(solution)/shard_map/dot_general | solution.py:194
  (67 shorter events, 2.0 us)
Async XLA Ops:
  6.5 1.3 copy-start
  6.5 71.8 %all-gather.3.cloned.1.call-start = ((), (), s32[]{:S(2)}) async-start(), calls=%async_computation.1 | async-start | bytes 2621440 | tf_op jit(solution)/shard_map/all_gather | solution.py:149
  55.8 78.3 %all-gather.5.cloned.1.call-start = ((), (), s32[]{:S(2)}) async-start(), calls=%async_computation.2 | async-start | bytes 2359296 | tf_op jit(solution)/shard_map/all_gather | solution.py:188
  58.0 24.8 %copy-start.3 = (f32[64]{0:T(128)S(1)}, f32[64]{0:T(128)}, u32[]{:S(2)}) copy-start(f32[64]{0:T(128)} %param.28) | copy-start | bytes 772
  58.0 24.9 %copy-start.4 = (f32[64]{0:T(128)S(1)}, f32[64]{0:T(128)}, u32[]{:S(2)}) copy-start(f32[64]{0:T(128)} %param.27) | copy-start | bytes 772
  58.0 25.0 %copy-start.1 = (bf16[64,2048]{1,0:T(8,128)(2,1)S(1)}, bf16[64,2048]{1,0:T(8,128)(2,1)}, u32[]{:S(2)}) copy-start(bf16[64,2048]{1,0:T(8,128)(2,1)} %param.17) | copy-start | bytes 786436
  58.1 25.0 %copy-start.2 = (f32[2048]{0:T(1024)S(1)}, f32[2048]{0:T(1024)}, u32[]{:S(2)}) copy-start(f32[2048]{0:T(1024)} %param.20) | copy-start | bytes 24580
  58.1 25.0 %copy-start.5 = (bf16[2048,128]{1,0:T(8,128)(2,1)S(1)}, bf16[2048,128]{1,0:T(8,128)(2,1)}, u32[]{:S(2)}) copy-start(bf16[2048,128]{1,0:T(8,128)(2,1)} %param.26) | copy-start | bytes 1572868
  58.1 25.0 %copy-start.6 = (bf16[2048,128]{1,0:T(8,128)(2,1)S(1)}, bf16[2048,128]{1,0:T(8,128)(2,1)}, u32[]{:S(2)}) copy-start(bf16[2048,128]{1,0:T(8,128)(2,1)} %param.25) | copy-start | bytes 1572868
  185.1 9.4 %all-to-all-start = ((bf16[4,128,256]{1,2,0:T(8,128)(2,1)}), bf16[4,128,256]{1,2,0:T(8,128)(2,1)S(1)}, u32[]{:S(2)}, u32[]{:S(2)}) async-start(bf16[4,128,256]{1,2,0:T(8,128)(2,1)} %copy.51), calls=%async_computation | async-start | bytes 524288 | tf_op jit(solution)/shard_map/all_to_all | solution.py:195
Sparse Core Ops, SparseCore 0:
  55.9 22.4 all-gather.2
  83.0 51.0 all-gather.4
where the time goes:
time: 206 us; the launch traced here: 205 us
  blocking collectives  74.3 us (36%)
  matrix products  43.6 us (21%)
  waiting for transfers between devices  41.2 us (20%)
  other arithmetic  24.3 us (12%)
  between operations  13.8 us (7%)
  local copies, waits for them, and re-layouts  4.5 us (2%)
  starting transfers between devices  3.45 us (2%)
    psum x1, blocking collectives, on_device(): lax.psum((widen(part_shift), widen(part_scale), widen(part_gate)), ('sp',...  42.4 us
    all_gather x1, blocking collectives, on_device(): ctx_whole = lax.all_gather(ctx_pairs, 'sp', axis=0, tiled=True)  31.9 us
    all_gather x1, waiting for transfers between devices, on_device(): lax.all_gather(hidden, 'tp', axis=0, tiled=True)  20.3 us
    reduce_sum x3, other arithmetic, process_probe_group(): row_total = row_total * shrink + jnp.sum(shares, axis=-1)  17.9 us
    dot_general x3, matrix products, process_probe_group(): jnp.einsum('dmvk,hmk->dmvh', probe_entries, matcher_pieces, preferred_ele...  17 us
    dot_general x3, matrix products, process_probe_group(): jnp.einsum('qkgn,nkd->qkgd', shares.astype(jnp.bfloat16), value_rows, pre...  15.7 us
    all_gather x1, waiting for transfers between devices, on_device(): key_piece = lax.all_gather(own_pairs, 'sp', axis=0, tiled=True)  15 us
    all_to_all x1, waiting for transfers between devices, on_device(): lax.all_to_all(attended, 'tp', split_axis=0, concat_axis=1, tiled=True)  5.96 us
  transfers between devices with their start and end apart: 3, of which 3 were waited for; matrix products, arithmetic and copies ran while one was open for 3% of the time, Pallas kernels for 0%

commit v1 on v0

--- a/solution.py
+++ b/solution.py
@@ -146,7 +146,9 @@
     kv_width = kv_heads * CHANNEL_SPAN
     joined_weight = jnp.concatenate([query_weight, key_weight, value_weight], axis=1)
     projected = jnp.dot(
-        lax.all_gather(hidden, "tp", axis=0, tiled=True),
+        jnp.concatenate(
+            lax.all_to_all(jnp.stack([hidden] * lax.axis_size("tp")), "tp", 0, 0), axis=0
+        ),
         joined_weight,
         preferred_element_type=jnp.float32,
     )

time: 206 us -> 214 us (1.039)
  starting transfers between devices: 3.45 us -> 7.05 us
  waiting for transfers between devices: 41.2 us -> 43.9 us
  local copies, waits for them, and re-layouts: 4.5 us -> 6.76 us
    all_to_all x0 -> x1, waiting for transfers between devices: none -> 25 us  [on_device(): lax.all_to_all(jnp.stack([hidden] * lax.axis_size('tp')), 'tp', 0, 0)]
    all_gather x1 -> x0, waiting for transfers between devices: 20.3 us -> none  [on_device(): lax.all_gather(hidden, 'tp', axis=0, tiled=True)]
    all_to_all x0 -> x1, starting transfers between devices: none -> 3.61 us  [on_device(): lax.all_to_all(jnp.stack([hidden] * lax.axis_size('tp')), 'tp', 0, 0)]
where the time goes in v1:
time: 214 us; the launch traced here: 213 us
  blocking collectives  74.6 us (35%)
  matrix products  44.3 us (21%)
  waiting for transfers between devices  43.9 us (21%)
  other arithmetic  23.1 us (11%)
  between operations  13.7 us (6%)
  starting transfers between devices  7.05 us (3%)
  local copies, waits for them, and re-layouts  6.76 us (3%)
    psum x1, blocking collectives, on_device(): lax.psum((widen(part_shift), widen(part_scale), widen(part_gate)), ('sp',...  43 us
    all_gather x1, blocking collectives, on_device(): ctx_whole = lax.all_gather(ctx_pairs, 'sp', axis=0, tiled=True)  31.6 us
    all_to_all x1, waiting for transfers between devices, on_device(): lax.all_to_all(jnp.stack([hidden] * lax.axis_size('tp')), 'tp', 0, 0)  25 us
    reduce_sum x3, other arithmetic, process_probe_group(): row_total = row_total * shrink + jnp.sum(shares, axis=-1)  17.9 us
    dot_general x3, matrix products, process_probe_group(): jnp.einsum('dmvk,hmk->dmvh', probe_entries, matcher_pieces, preferred_ele...  17 us
    dot_general x3, matrix products, process_probe_group(): jnp.einsum('qkgn,nkd->qkgd', shares.astype(jnp.bfloat16), value_rows, pre...  15.7 us
    all_gather x1, waiting for transfers between devices, on_device(): key_piece = lax.all_gather(own_pairs, 'sp', axis=0, tiled=True)  12.9 us
    all_to_all x1, waiting for transfers between devices, on_device(): lax.all_to_all(attended, 'tp', split_axis=0, concat_axis=1, tiled=True)  5.95 us
  transfers between devices with their start and end apart: 3, of which 3 were waited for; matrix products, arithmetic and copies ran while one was open for 3% of the time, Pallas kernels for 0%

profile of v1, /device:TPU:0, one launch (start us, length us, event | category | flops | bytes accessed | tf_op | source)
XLA Modules:
  0.0 213.4 jit_solution(1958549437016337583)
XLA Ops:
  6.5 1.3 fusion.31
  7.8 0.9 convolution_dynamic-update-slice_fusion.1
  8.8 1.2 convolution_dynamic-update-slice_fusion
  10.0 1.2 convolution_dynamic-update-slice_fusion.2
  11.2 43.0 %all-reduce = (f32[2,2048]{1,0:T(2,128)S(1)}, f32[2,2048]{1,0:T(2,128)S(1)}, f32[2,2048]{1,0:T(2,128)}) all-reduce(f32[2,2048]{1,0:T(2,128)S(1)} %convolution_dynamic-update-slice_fusion, f32[2,2048]{1,0:T(2,128)S(1)} %convolution_dynamic-update-slice_fusion.1, ...), channel_id=1, replica_groups=mesh['sp'=8,'tp'=4] {'sp','tp'}, use_global_device_ids=true, to_apply=%region_3.4 | all-reduce | flops 12288 | bytes 98304 | tf_op jit(solution)/shard_map/psum | solution.py:134
  54.2 0.6 slice_add_fusion
  54.8 1.3 fusion.35
  56.1 1.6 stack.19
  57.7 3.6 %all-to-all-start = ((bf16[4,128,2048]{2,1,0:T(8,128)(2,1)}), bf16[4,128,2048]{2,1,0:T(8,128)(2,1)S(1)}, u32[]{:S(2)}, u32[]{:S(2)}) async-start(bf16[4,128,2048]{2,1,0:T(8,128)(2,1)} %stack.19), calls=%async_computation | async-start | bytes 4194304 | tf_op jit(solution)/shard_map/all_to_all | solution.py:150
  62.0 25.0 %all-to-all-done = bf16[4,128,2048]{2,1,0:T(8,128)(2,1)S(1)} async-done(((bf16[4,128,2048]{2,1,0:T(8,128)(2,1)}), bf16[4,128,2048]{2,1,0:T(8,128)(2,1)S(1)}, u32[]{:S(2)}, u32[]{:S(2)}) %all-to-all-start) | async-done | bytes 2097184 | tf_op jit(solution)/shard_map/all_to_all | solution.py:150
  87.0 2.8 %fusion.17 = f32[512,512]{0,1:T(8,128)S(1)} fusion(bf16[512,2048]{1,0:T(8,128)(2,1)S(1)} %bitcast.123, bf16[2048,128]{1,0:T(8,128)(2,1)} %param.26, bf16[2048,128]{1,0:T(8,128)(2,1)} %param.25, bf16[2048,256]{1,0:T(8,128)(2,1)} %param.24), kind=kOutput, calls=%fused_computation.22 | convolution fusion | flops 1080033280 | bytes 5242880 | tf_op jit(solution)/shard_map/dot_general | solution.py:148
  90.1 0.7 pad_maximum_fusion.1
  90.9 0.7 mul.336
  91.6 0.7 mul.352
  92.3 1.7 fusion.36
  94.6 31.6 %all_gather.6 = bf16[512,256]{1,0:T(8,128)(2,1)S(1)} all-gather(bf16[64,256]{1,0:T(8,128)(2,1)S(1)} %pad_maximum_fusion.4), channel_id=1, replica_groups=mesh['sp'=8,'tp'=4] {'sp'}, dimensions={0}, use_global_device_ids=true | all-gather | bytes 294912 | tf_op jit(solution)/shard_map/all_gather | solution.py:183
  126.8 0.8 bitcast_reduce_fusion.1
  127.5 0.8 fusion.14
  128.4 1.0 fusion.28
  129.4 12.9 %all-gather.2.cloned.1.call-done = bf16[4096,256]{0,1:T(8,128)(2,1)} async-done(((bf16[512,256]{0,1:T(8,128)(2,1)}), bf16[4096,256]{0,1:T(8,128)(2,1)}) %all-gather.2.cloned.1.call-update) | async-done | bytes 2097168 | tf_op jit(solution)/shard_map/all_gather | solution.py:190
  142.3 1.7 copy.61
  144.1 48.4 %while.14 = (s32[]{:T(128)}, f32[512,2,2]{0,2,1:T(2,128)S(1)}, f32[512,2,2]{0,2,1:T(2,128)S(1)}, f32[512,2,2,64]{0,3,2,1:T(8,128)S(1)}, bf16[2,2048,256]{1,2,0:T...) while((s32[]{:T(128)}, f32[512,2,2]{0,2,1:T(2,128)S(1)}, f32[512,2,2]{0,2,1:T(2,128)S(1)}, ...), condition=%wide.region_13.14_spmd, body=%wide.region_10.13_spmd.sunk | while | flops 1107562496 | bytes 57016408 | solution.py:88
  144.3 8.1 %bitcast_reduce_fusion.5 = (f32[512,2,2]{0,2,1:T(2,128)S(1)}, f32[2,2048,512,2]{2,1,3,0:T(8,128)}) fusion(bf16[2048,2,64,1]{0,2,3,1:T(8,128)(2,1)S(1)} %bitcast.117, bf16[512,2,2,64]{0,3,2,1:T(8,128)(2,1)S(1)} %get-tuple-element.187), kind=kOutput, calls=%fused_computation.1.clone.1 | convolution fusion | flops 545257472 | bytes 17571840 | tf_op jit(solution)/shard_map/while/body/eval_jaxpr/dmvk,hmk->dmvh/dot_general | solution.py:55
  152.4 8.5 %fusion.94 = f32[512,2,2]{0,2,1:T(2,128)S(1)} fusion(f32[2,2048,512,2]{2,1,3,0:T(8,128)} %get-tuple-element.164, f32[512,2,2]{0,2,1:T(2,128)S(1)} %max.4), kind=kLoop, calls=%fused_computation.4.clone.1 | loop fusion | flops 12580864 | bytes 16793600 | tf_op jit(solution)/shard_map/while/body/eval_jaxpr/reduce_sum | solution.py:64
  160.9 7.3 %fusion.95 = f32[512,2,2,64]{0,3,2,1:T(8,128)S(1)} fusion(bf16[2048,2,64,1]{0,2,3,1:T(8,128)(2,1)S(1)} %bitcast.118, f32[2,2048,512,2]{2,1,3,0:T(8,128)} %get-tuple-element.164, f32[512,2,2]{0,2,1:T(2,128)S(1)} %max.4, f32[512,2,2,64]{0,3,2,1:T(8,128)S(1)} %get-tuple-element.178, f32[512,2,2]{0,2,1:T(2,128)S(1)} %get-tuple-element.167), kind=kOutput, calls=%fused_computation.7.clone.1 | convolution fusion | flops 549715968 | bytes 18366464 | tf_op jit(solution)/shard_map/while/body/eval_jaxpr/qkgn,nkd->qkgd/dot_general | solution.py:65
  168.5 8.1 %bitcast_reduce_fusion.5 = (f32[512,2,2]{0,2,1:T(2,128)S(1)}, f32[2,2048,512,2]{2,1,3,0:T(8,128)}) fusion(bf16[2048,2,64,1]{0,2,3,1:T(8,128)(2,1)S(1)} %bitcast.117, bf16[512,2,2,64]{0,3,2,1:T(8,128)(2,1)S(1)} %get-tuple-element.187), kind=kOutput, calls=%fused_computation.1.clone.1 | convolution fusion | flops 545257472 | bytes 17571840 | tf_op jit(solution)/shard_map/while/body/eval_jaxpr/dmvk,hmk->dmvh/dot_general | solution.py:55
  176.6 8.5 %fusion.94 = f32[512,2,2]{0,2,1:T(2,128)S(1)} fusion(f32[2,2048,512,2]{2,1,3,0:T(8,128)} %get-tuple-element.164, f32[512,2,2]{0,2,1:T(2,128)S(1)} %max.4), kind=kLoop, calls=%fused_computation.4.clone.1 | loop fusion | flops 12580864 | bytes 16793600 | tf_op jit(solution)/shard_map/while/body/eval_jaxpr/reduce_sum | solution.py:64
  185.1 7.3 %fusion.95 = f32[512,2,2,64]{0,3,2,1:T(8,128)S(1)} fusion(bf16[2048,2,64,1]{0,2,3,1:T(8,128)(2,1)S(1)} %bitcast.118, f32[2,2048,512,2]{2,1,3,0:T(8,128)} %get-tuple-element.164, f32[512,2,2]{0,2,1:T(2,128)S(1)} %max.4, f32[512,2,2,64]{0,3,2,1:T(8,128)S(1)} %get-tuple-element.178, f32[512,2,2]{0,2,1:T(2,128)S(1)} %get-tuple-element.167), kind=kOutput, calls=%fused_computation.7.clone.1 | convolution fusion | flops 549715968 | bytes 18366464 | tf_op jit(solution)/shard_map/while/body/eval_jaxpr/qkgn,nkd->qkgd/dot_general | solution.py:65
  192.6 0.7 copy.51
  193.4 3.4 %all-to-all-start.1 = ((bf16[4,128,256]{1,2,0:T(8,128)(2,1)}), bf16[4,128,256]{1,2,0:T(8,128)(2,1)S(1)}, u32[]{:S(2)}, u32[]{:S(2)}) async-start(bf16[4,128,256]{1,2,0:T(8,128)(2,1)} %copy.51), calls=%async_computation.1 | async-start | bytes 524288 | tf_op jit(solution)/shard_map/all_to_all | solution.py:197
  196.8 5.9 %all-to-all-done.1 = bf16[4,128,256]{1,2,0:T(8,128)(2,1)S(1)} async-done(((bf16[4,128,256]{1,2,0:T(8,128)(2,1)}), bf16[4,128,256]{1,2,0:T(8,128)(2,1)S(1)}, u32[]{:S(2)}, u32[]{:S(2)}) %all-to-all-start.1) | async-done | bytes 262176 | tf_op jit(solution)/shard_map/all_to_all | solution.py:197
  202.8 3.8 %fusion.16 = bf16[128,2048]{1,0:T(8,128)(2,1)} fusion(bf16[128,1024]{0,1:T(8,128)(2,1)S(1)} %bitcast.126, bf16[1024,2048]{1,0:T(8,128)(2,1)} %param.29, bf16[128,2048]{1,0:T(8,128)(2,1)} %param.16, f32[2048]{0:T(1024)S(1)} %bitcast.136), kind=kOutput, calls=%fused_computation.20 | convolution fusion | flops 537919488 | bytes 5513216 | tf_op jit(solution)/shard_map/dot_general | solution.py:196
  (63 shorter events, 2.6 us)
Async XLA Ops:
  6.5 1.3 copy-start
  9.9 51.4 %copy-start.4 = (f32[64]{0:T(128)S(1)}, f32[64]{0:T(128)}, u32[]{:S(2)}) copy-start(f32[64]{0:T(128)} %param.28) | copy-start | bytes 772
  11.2 50.7 %copy-start.1 = (bf16[64,2048]{1,0:T(8,128)(2,1)S(1)}, bf16[64,2048]{1,0:T(8,128)(2,1)}, u32[]{:S(2)}) copy-start(bf16[64,2048]{1,0:T(8,128)(2,1)} %param.17) | copy-start | bytes 786436
  57.7 29.2 %all-to-all-start = ((bf16[4,128,2048]{2,1,0:T(8,128)(2,1)}), bf16[4,128,2048]{2,1,0:T(8,128)(2,1)S(1)}, u32[]{:S(2)}, u32[]{:S(2)}) async-start(bf16[4,128,2048]{2,1,0:T(8,128)(2,1)} %stack.19), calls=%async_computation | async-start | bytes 4194304 | tf_op jit(solution)/shard_map/all_to_all | solution.py:150
  61.3 81.0 %all-gather.2.cloned.1.call-start = ((), (), s32[]{:S(2)}) async-start(), calls=%async_computation.2 | async-start | bytes 2359296 | tf_op jit(solution)/shard_map/all_gather | solution.py:190
  87.0 5.4 %copy-start.2 = (f32[2048]{0:T(1024)S(1)}, f32[2048]{0:T(1024)}, u32[]{:S(2)}) copy-start(f32[2048]{0:T(1024)} %param.20) | copy-start | bytes 24580
  144.1 52.7 %copy-start.3 = (f32[2,2048]{1,0:T(2,128)S(1)}, f32[2,2048]{1,0:T(2,128)}, u32[]{:S(2)}) copy-start(f32[2,2048]{1,0:T(2,128)} %get-tuple-element.90) | copy-start | bytes 49156
  193.4 9.4 %all-to-all-start.1 = ((bf16[4,128,256]{1,2,0:T(8,128)(2,1)}), bf16[4,128,256]{1,2,0:T(8,128)(2,1)S(1)}, u32[]{:S(2)}, u32[]{:S(2)}) async-start(bf16[4,128,256]{1,2,0:T(8,128)(2,1)} %copy.51), calls=%async_computation.1 | async-start | bytes 524288 | tf_op jit(solution)/shard_map/all_to_all | solution.py:197
Sparse Core Ops, SparseCore 0:
  91.0 51.3 all-gather.1
